TPU v7x, 512 devices: a whole 4x8x8 slice. The times are simulated.
512 devices in a mesh: ep: 32 (over z, x), tp: 16 (over y, core).
Axes of the slice: x: 4, y: 8, z: 8, core: 2. Of those that a mesh axis runs over, the one named last changes fastest.
Arguments:
- query_latent: bfloat16 [8192, 768], P('ep'), may hold values from -600 to 600
- shared_latent: bfloat16 [8192, 512], P('ep'), may hold values from -600 to 600
- rotary_key: bfloat16 [8192, 64], P('ep'), may hold values from -2500 to 2500
- query_gain: float32 [768], replicated, may hold values from 0.1 to 1.9
- shared_gain: float32 [512], replicated, may hold values from 0.1 to 1.9
- query_plain_weight: bfloat16 [768, 2048], P(None, 'tp'), may hold values from -0.21875 to 0.21875
- query_turn_weight: bfloat16 [768, 1024], P(None, 'tp'), may hold values from -0.21875 to 0.21875
- key_weight: bfloat16 [512, 2048], P(None, 'tp'), may hold values from -0.25 to 0.25
- value_weight: bfloat16 [512, 2048], P(None, 'tp'), may hold values from -0.25 to 0.25
- mixer_out_weight: bfloat16 [2048, 2048], P('tp'), may hold values from -1 to 1
- expert_input: bfloat16 [4096, 2048], P('ep'), may hold values from -600 to 600
- expert_gain: float32 [2048], replicated, may hold values from 0.1 to 1.9
- routing: int32 [4096, 4], P('ep'), may hold values from 0 to 31, all different within a row; in each aligned block of 128 rows (0 to 127, 128 to 255, ...) at most 21 rows name the same one
- routing_weight: float32 [4096, 4], P('ep'), may hold values from 0.05 to 1
- gate_weight: bfloat16 [32, 2048, 2048], P('ep', None, 'tp'), may hold values from -0.375 to 0.375
- up_weight: bfloat16 [32, 2048, 2048], P('ep', None, 'tp'), may hold values from -0.375 to 0.375
- down_weight: bfloat16 [32, 2048, 2048], P('ep', 'tp'), may hold values from -0.01953125 to 0.01953125
Outputs:
- mixer_output: bfloat16 [8192, 2048], P('ep')
- expert_output: bfloat16 [4096, 2048], P('ep')
Inputs may be any that keep to these rules, and one draw needn't show every extreme that they name: `routing`: each row names 4 different experts. In each aligned block of 128 rows (the rows of one index of ep) no expert is named by more than 21 rows, and in some block some expert is named by exactly 21.
All inputs are finite; a program needn't handle non-finite values.
Results may differ from a plain program's by a relative error of at most 0.019.
Values may be sent and summed in bfloat16 or wider, within the bound.
A program may use at most 128 MiB of HBM per device.

v0:
```python
import jax
import jax.numpy as jnp
from jax import lax
from jax.sharding import Mesh
from jax.sharding import PartitionSpec as P

NOPE = 128
ROPE = 64
VDIM = 128
TP = ("tp_0", "tp_1")
EPSILON = 1e-06
CLAMP_LIMIT = 7.0
SLOPE = 1.702
ROTARY_BASE = 10000.0
NEGATIVE = -1e30


def sent_together(arrays, axis, dim, along):
    columns = [a.reshape(*a.shape[:along], -1) for a in arrays]
    both = jnp.concatenate(columns, axis=along)
    out, at, done = (lax.all_gather(both, axis, axis=dim, tiled=True), 0, [])
    for a, column in zip(arrays, columns):
        share = out[..., at : at + column.shape[along]]
        done.append(share.reshape(*share.shape[:along], *a.shape[along:]))
        at += column.shape[along]
    return tuple(done)


def padded_to(lines, length):
    spare = -len(lines) % length
    return jnp.pad(lines, [(0, spare)] + [(0, 0)] * (lines.ndim - 1))


def sum_in_order(pieces, axes, turns):
    inside = pieces.shape[1:]
    pieces = pieces.reshape(*(lax.axis_size(a) for a in axes), *inside)
    pieces = jnp.moveaxis(pieces, turns, range(len(axes))).reshape(-1, *inside)
    for k in turns:
        pieces = lax.psum_scatter(pieces, axes[k], scatter_dimension=0, tiled=True)
    return pieces[0]


def gather_in_order(shard, axes, turns):
    pieces = shard[None]
    for k in turns:
        pieces = lax.all_gather(pieces, axes[k], axis=0, tiled=True)
    block = [lax.axis_size(axes[k]) for k in reversed(turns)]
    pieces = pieces.reshape(*block, *shard.shape)
    turned = sorted(range(len(turns)), key=lambda place: turns[len(turns) - 1 - place])
    return pieces.transpose(*turned, *range(len(turns), pieces.ndim)).reshape(-1, *shard.shape)


def sum_by_parts(shard, axes, turns):
    length, lines = (lax.axis_size(axes), shard.reshape(-1, *shard.shape[1:][-1:]))
    pieces = padded_to(lines, length).reshape(length, -1, *lines.shape[1:])
    own = sum_in_order(pieces, axes, turns)
    whole = gather_in_order(own, axes, turns[::-1]).reshape(-1, *lines.shape[1:])
    return whole[: len(lines)].reshape(shard.shape)


def sum_by_parts_2(shard, axis):
    lines = shard.reshape(-1, *shard.shape[1:][-1:])
    padded = padded_to(lines, lax.axis_size(axis))
    own = lax.psum_scatter(padded, axis, scatter_dimension=0, tiled=True)
    whole = lax.all_gather(own, axis, axis=0, tiled=True)
    return whole[: len(lines)].reshape(shard.shape)


def norm_rows(values, gains):
    widened = values.astype(jnp.float32)
    normed = widened * lax.rsqrt(jnp.mean(widened * widened, axis=-1, keepdims=True) + EPSILON)
    return (normed * gains).astype(jnp.bfloat16)


def rotary(values, position):
    half_dim = values.shape[-1] // 2
    frequency = ROTARY_BASE ** (-2.0 * jnp.arange(half_dim, dtype=jnp.float32) / values.shape[-1])
    angles = position.astype(jnp.float32)[:, None, None] * frequency[None, None, :]
    cosine = jnp.cos(angles)
    sine_part = jnp.sin(angles)
    lower = values[..., :half_dim]
    upper = values[..., half_dim:]
    return jnp.concatenate(
        [lower * cosine - upper * sine_part, upper * cosine + lower * sine_part], axis=-1
    )


def mixer_part(
    query_latent,
    shared_latent,
    rotary_key,
    query_gain,
    shared_gain,
    query_plain_weight,
    query_turn_weight,
    key_weight,
    value_weight,
    mixer_out_weight,
):
    row_count = query_latent.shape[0]
    head_count = query_plain_weight.shape[1] // NOPE
    position = lax.axis_index("ep") * row_count + jnp.arange(row_count, dtype=jnp.int32)
    query_normed = norm_rows(query_latent, query_gain)
    shared_normed = norm_rows(shared_latent, shared_gain)
    query_plain = jnp.dot(query_normed, query_plain_weight, preferred_element_type=jnp.float32)
    query_plain = query_plain.astype(jnp.bfloat16).reshape(row_count, head_count, NOPE)
    query_raw = jnp.dot(query_normed, query_turn_weight, preferred_element_type=jnp.float32)
    query_turned = rotary(query_raw.reshape(row_count, head_count, ROPE), position).astype(
        jnp.bfloat16
    )
    key_turned = rotary(rotary_key.astype(jnp.float32).reshape(row_count, 1, ROPE), position)
    key_turned = key_turned.astype(jnp.bfloat16).reshape(row_count, ROPE)
    scaling = (NOPE + ROPE) ** (-0.5)
    own_keys = jnp.dot(shared_normed, key_weight, preferred_element_type=jnp.float32)
    own_keys = own_keys.astype(jnp.bfloat16).reshape(row_count, head_count, NOPE)
    own_values = jnp.dot(shared_normed, value_weight, preferred_element_type=jnp.float32)
    own_values = own_values.astype(jnp.bfloat16).reshape(row_count, head_count, VDIM)
    portion = sent_together((own_keys, own_values, key_turned), "ep", 0, 1)
    key_plain = portion[0]
    key_total = key_plain.shape[0]
    peak_old = jnp.full((head_count, row_count), NEGATIVE, jnp.float32)
    scores = jnp.einsum("qhd,khd->hqk", query_plain, key_plain, preferred_element_type=jnp.float32)
    scores = scores + jnp.einsum(
        "qhr,kr->hqk", query_turned, portion[2], preferred_element_type=jnp.float32
    )
    scores = scores * scaling
    key_position = jnp.arange(key_total, dtype=jnp.int32)
    visible = (key_position[None, :] <= position[:, None])[None]
    scores = jnp.where(visible, scores, NEGATIVE)
    peak_new = jnp.maximum(peak_old, jnp.max(scores, axis=-1))
    weight = jnp.where(visible, jnp.exp(scores - peak_new[..., None]), 0.0)
    totals_new = jnp.sum(weight, axis=-1)
    accum_new = jnp.einsum(
        "hqk,khd->hqd", weight.astype(jnp.bfloat16), portion[1], preferred_element_type=jnp.float32
    )
    folded = (peak_new, totals_new, accum_new)
    peak_final, totals_final, accum_final = folded
    heads_out = accum_final / totals_final[..., None]
    heads_out = (
        jnp.transpose(heads_out, (1, 0, 2))
        .reshape(row_count, head_count * VDIM)
        .astype(jnp.bfloat16)
    )
    partial_value = jnp.dot(heads_out, mixer_out_weight, preferred_element_type=jnp.float32)
    return (
        sum_by_parts(partial_value.astype(jnp.bfloat16), TP, (0, 1))
        .astype(jnp.float32)
        .astype(jnp.bfloat16)
    )


def expert_part(
    expert_input, expert_gain, routing, routing_weight, gate_weight, up_weight, down_weight
):
    token_count = expert_input.shape[0]
    top_count = routing.shape[1]
    width = expert_input.shape[1]
    experts = lax.axis_size("ep")
    capacity = 4 * token_count * top_count // (3 * experts)
    normed = norm_rows(expert_input, expert_gain)
    flattened = routing.reshape(token_count * top_count)
    matches = (flattened[:, None] == jnp.arange(experts, dtype=jnp.int32)[None, :]).astype(
        jnp.int32
    )
    ranking = jnp.cumsum(matches, axis=0) - 1
    slot_index = jnp.sum(ranking * matches, axis=1)
    target = (flattened * capacity + slot_index).reshape(token_count, top_count)
    slot_ids = jnp.arange(experts * capacity, dtype=jnp.int32)
    select = target[None, :, :] == slot_ids[:, None, None]
    gather_table = jnp.any(select, axis=2).astype(jnp.bfloat16)
    outgoing = jnp.dot(gather_table, normed, preferred_element_type=jnp.float32).astype(
        jnp.bfloat16
    )
    outgoing = outgoing.reshape(experts, capacity, width)
    arrived = lax.all_to_all(outgoing, "ep", split_axis=0, concat_axis=0, tiled=True).reshape(
        experts * capacity, width
    )
    gate_local = gate_weight[0]
    up_local = up_weight[0]
    down_local = down_weight[0]
    gate_pre = jnp.minimum(
        jnp.dot(arrived, gate_local, preferred_element_type=jnp.float32), CLAMP_LIMIT
    )
    up_pre = jnp.clip(
        jnp.dot(arrived, up_local, preferred_element_type=jnp.float32), -CLAMP_LIMIT, CLAMP_LIMIT
    )
    hidden = ((up_pre + 1.0) * (gate_pre * jax.nn.sigmoid(SLOPE * gate_pre))).astype(jnp.bfloat16)
    partial_value = jnp.dot(hidden, down_local, preferred_element_type=jnp.float32)
    summed = sum_by_parts_2(partial_value.astype(jnp.bfloat16), TP).astype(jnp.float32)
    summed = summed.astype(jnp.bfloat16).reshape(experts, capacity, width)
    returned_rows = lax.all_to_all(summed, "ep", split_axis=0, concat_axis=0, tiled=True).reshape(
        experts * capacity, width
    )
    mixing = jnp.transpose(jnp.sum(jnp.where(select, routing_weight[None, :, :], 0.0), axis=2))
    result = jnp.dot(mixing, returned_rows.astype(jnp.float32))
    return result.astype(jnp.bfloat16)


def per_device(
    query_latent,
    shared_latent,
    rotary_key,
    query_gain,
    shared_gain,
    query_plain_weight,
    query_turn_weight,
    key_weight,
    value_weight,
    mixer_out_weight,
    expert_input,
    expert_gain,
    routing,
    routing_weight,
    gate_weight,
    up_weight,
    down_weight,
):
    mixer_output = mixer_part(
        query_latent,
        shared_latent,
        rotary_key,
        query_gain,
        shared_gain,
        query_plain_weight,
        query_turn_weight,
        key_weight,
        value_weight,
        mixer_out_weight,
    )
    expert_output = expert_part(
        expert_input, expert_gain, routing, routing_weight, gate_weight, up_weight, down_weight
    )
    return (mixer_output, expert_output)


def solution(mesh):
    finer = Mesh(mesh.devices.reshape(mesh.shape["ep"], 8, 2), ("ep", "tp_0", "tp_1"))
    placed = (
        P("ep", None),
        P("ep", None),
        P("ep", None),
        P(),
        P(),
        P(None, TP),
        P(None, TP),
        P(None, TP),
        P(None, TP),
        P(TP, None),
        P("ep", None),
        P(),
        P("ep", None),
        P("ep", None),
        P("ep", None, TP),
        P("ep", None, TP),
        P("ep", TP, None),
    )
    return jax.shard_map(
        per_device,
        mesh=finer,
        in_specs=placed,
        out_specs=(P("ep", None), P("ep", None)),
        check_vma=False,
    )
```

profile of v0, /device:TPU:2, one launch (start us, length us, event | category | flops | bytes accessed | tf_op | source)
XLA Modules:
  0.0 364.6 jit_solution(4953756799054424215)
XLA Ops:
  7.3 1.2 fusion.33
  8.5 0.8 bitcast_convert_fusion
  9.3 1.1 fusion.36
  10.4 1.3 convolution_convert_fusion.4
  11.7 1.3 convolution_convert_fusion.5
  13.0 1.3 convolution_bitcast_fusion.2
  14.3 0.3 fusion.85
  14.6 0.7 pad_maximum_fusion
  15.3 0.8 copy.44
  16.1 0.1 eq.42
  16.2 0.1 eq.38
  16.3 1.2 reduce-window.6
  17.5 0.2 slice_reduce_fusion
  17.8 0.1 fusion.62
  17.9 0.1 reduce_sum.60
  18.0 0.1 copy.47
  18.1 0.7 multiply_add_fusion
  18.8 0.2 fusion.29
  19.0 0.2 fusion.11
  19.1 2.0 convolution_convert_fusion.1
  21.1 2.5 reshape.278
  23.7 97.5 %all_to_all.10 = bf16[32,21,2048]{2,1,0:T(8,128)(2,1)} all-to-all(bf16[32,21,2048]{2,1,0:T(8,128)(2,1)} %reshape.278), channel_id=1, replica_groups=mesh['ep'=32,'tp_0'=8,'tp_1'=2] {'ep'}, dimensions={0} | all-to-all | bytes 5505024 | tf_op jit(solution)/shard_map/all_to_all | solution.py:175
  121.1 3.1 reshape.279
  124.2 2.6 convolution_minimum_fusion
  126.8 5.7 %convolution_convert_fusion = bf16[672,2048]{1,0:T(8,128)(2,1)} fusion(bf16[672,2048]{1,0:T(8,128)(2,1)S(1)} %reshape.279, bf16[1,128,2048]{2,1,0:T(8,128)(2,1)S(1)} %copy-done, bf16[1,2048,128]{2,1,0:T(8,128)(2,1)} %param.32, f32[672,128]{1,0:T(8,128)} %convolution_minimum_fusion), kind=kOutput, calls=%fused_computation.11 | convolution fusion | flops 706793472 | bytes 6897664 | tf_op jit(solution)/shard_map/dot_general | solution.py:188
  132.5 35.4 %fusion = bf16[48,2048]{1,0:T(8,128)(2,1)S(1)} fusion(bf16[672,2048]{1,0:T(8,128)(2,1)} %convolution_convert_fusion), kind=kCustom, calls=%all-reduce-scatter | all-reduce-scatter fusion | flops 1572865 | bytes 2951168
  167.9 1.3 collective-permute-start
  169.3 1.3 collective-permute-start.1
  170.6 1.3 dynamic-slice.4
  172.5 2.1 collective-permute-done.1
  174.6 0.8 concatenate.30
  175.4 0.7 dynamic-slice_bitcast_fusion
  176.2 6.3 %convolution_bitcast_fusion.1 = f32[1,256,8192]{2,1,0:T(8,128)} fusion(bf16[8192,320]{0,1:T(8,128)(2,1)} %all-gather.5.cloned.1.call-done, bf16[768,128]{1,0:T(8,128)(2,1)S(1)} %copy-done.3, bf16[256,768]{1,0:T(8,128)(2,1)S(1)} %copy-done.2, f32[768]{0:T(1024)S(1)} %copy-done.5, f32[256]{0:T(256)S(1)} %add_rsqrt_fusion.1), kind=kOutput, calls=%fused_computation.1 | convolution fusion | flops 588021760 | bytes 11079680 | tf_op jit(solution)/shard_map/qhd,khd->hqk/dot_general | solution.py:122
  182.5 6.9 %fusion.96 = (f32[256]{0:T(256)S(1)}, f32[1,256,8192]{2,1,0:T(8,128)}) fusion(f32[1,256,8192]{2,1,0:T(8,128)} %convolution_bitcast_fusion.1, bf16[256,32]{0,1:T(8,128)(2,1)S(1)} %get-tuple-element.3, bf16[256,32]{0,1:T(8,128)(2,1)S(1)} %get-tuple-element.2, bf16[8192,320]{0,1:T(8,128)(2,1)} %all-gather.5.cloned.1.call-done, s32[256]{0:T(256)S(1)} %iota_add_fusion), kind=kOutput, calls=%fused_computation.113 | convolution fusion | flops 278986496 | bytes 17860608 | tf_op jit(solution)/shard_map/qhr,kr->hqk/dot_general | solution.py:123
  189.4 30.8 %all-gather.9.cloned.1.call-done = bf16[16,42,2048]{2,1,0:T(8,128)(2,1)} async-done(((bf16[1,42,2048]{2,1,0:T(8,128)(2,1)}), bf16[16,42,2048]{2,1,0:T(8,128)(2,1)}) %all-gather.9.cloned.1.call-update) | async-done | bytes 2752528 | tf_op jit(solution)/shard_map/all_gather | solution.py:65
  220.2 5.3 %reshape.280 = bf16[32,21,2048]{2,1,0:T(8,128)(2,1)} reshape(bf16[16,42,2048]{2,1,0:T(8,128)(2,1)} %all-gather.9.cloned.1.call-done) | data formatting | bytes 5505024 | tf_op jit(solution)/shard_map/reshape | solution.py:190
  225.6 10.6 %all-to-all-start.1 = ((bf16[32,21,2048]{2,1,0:T(8,128)(2,1)}), bf16[32,21,2048]{2,1,0:T(8,128)(2,1)}, u32[]{:S(2)}, u32[]{:S(2)}) async-start(bf16[32,21,2048]{2,1,0:T(8,128)(2,1)} %reshape.280), calls=%async_computation.3 | async-start | bytes 6291456 | tf_op jit(solution)/shard_map/all_to_all | solution.py:191
  236.1 0.2 reduce-scatter.5.cloned.1.call-start
  236.4 4.7 %fusion.4 = f32[256]{0:T(256)S(1)} fusion(f32[1,256,8192]{2,1,0:T(8,128)} %get-tuple-element.9, f32[256]{0:T(256)S(1)} %broadcast_maximum_fusion, s32[256]{0:T(256)S(1)} %iota_add_fusion), kind=kLoop, calls=%fused_computation.7 | loop fusion | flops 8388352 | bytes 8391680 | tf_op jit(solution)/shard_map/reduce_sum | solution.py:132
  241.0 7.5 %convolution_convert_fusion.2 = bf16[256,2048]{1,0:T(8,128)(2,1)} fusion(bf16[128,2048]{1,0:T(8,128)(2,1)S(1)} %copy-done.7, bf16[8192,320]{0,1:T(8,128)(2,1)} %all-gather.5.cloned.1.call-done, f32[1,256,8192]{2,1,0:T(8,128)} %get-tuple-element.9, f32[256]{0:T(256)S(1)} %broadcast_maximum_fusion, s32[256]{0:T(256)S(1)} %iota_add_fusion, f32[256]{0:T(256)S(1)} %fusion.4), kind=kOutput, calls=%fused_computation.13 | convolution fusion | flops 680067072 | bytes 12061696 | tf_op jit(solution)/shard_map/dot_general | solution.py:144
  248.6 39.5 %reduce-scatter.5.cloned.1.call-done = bf16[2,16,2048]{2,1,0:T(8,128)(2,1)} async-done(((bf16[16,16,2048]{2,1,0:T(8,128)(2,1)}), bf16[2,16,2048]{2,1,0:T(8,128)(2,1)}) %reduce-scatter.5.cloned.1.call-update) | async-done | bytes 131088 | tf_op jit(solution)/shard_map/reduce_scatter | solution.py:39
  288.2 17.4 %reduce-scatter.7.cloned.1.call-done = bf16[1,16,2048]{2,1,0:T(8,128)(2,1)} async-done(((bf16[2,16,2048]{2,1,0:T(8,128)(2,1)}), bf16[1,16,2048]{2,1,0:T(8,128)(2,1)}) %reduce-scatter.7.cloned.1.call-update) | async-done | bytes 65552 | tf_op jit(solution)/shard_map/reduce_scatter | solution.py:39
  305.5 3.5 all_gather.13
  309.1 0.1 select_reduce_fusion
  309.3 42.1 %all-gather.7.cloned.1.call-done = bf16[16,16,2048]{2,1,0:T(8,128)(2,1)} async-done(((bf16[2,16,2048]{2,1,0:T(8,128)(2,1)}), bf16[16,16,2048]{2,1,0:T(8,128)(2,1)}) %all-gather.7.cloned.1.call-update) | async-done | bytes 1048592 | tf_op jit(solution)/shard_map/all_gather | solution.py:46
  351.3 3.0 reshape.281
  354.4 1.4 fusion.97
  355.8 2.3 copy.52
  (39 shorter events, 0.5 us)
Async XLA Ops:
  7.2 119.7 %copy-start = (bf16[1,128,2048]{2,1,0:T(8,128)(2,1)S(1)}, bf16[1,128,2048]{2,1,0:T(8,128)(2,1)}, u32[]{:S(2)}) copy-start(bf16[1,128,2048]{2,1,0:T(8,128)(2,1)} %param.33) | copy-start | bytes 1572868
  7.2 11.6 %copy-start.1 = (bf16[128,2048]{1,0:T(8,128)(2,1)S(1)}, bf16[128,2048]{1,0:T(8,128)(2,1)}, u32[]{:S(2)}) copy-start(bf16[128,2048]{1,0:T(8,128)(2,1)} %param.27) | copy-start | bytes 1572868
  7.2 11.9 %copy-start.4 = (f32[2048]{0:T(1024)S(1)}, f32[2048]{0:T(1024)}, u32[]{:S(2)}) copy-start(f32[2048]{0:T(1024)} %param.28) | copy-start | bytes 24580
  7.2 169.0 %all-gather.5.cloned.1.call-start = ((), (), s32[]{:S(2)}) async-start(), calls=%async_computation.4 | async-start | bytes 5406720 | tf_op jit(solution)/shard_map/all_gather | solution.py:21
  15.3 204.9 %all-gather.9.cloned.1.call-start = ((), (), s32[]{:S(2)}) async-start(), calls=%async_computation.8 | async-start | bytes 3342336 | tf_op jit(solution)/shard_map/all_gather | solution.py:65
  132.5 43.7 %copy-start.2 = (bf16[256,768]{1,0:T(8,128)(2,1)S(1)}, bf16[256,768]{1,0:T(8,128)(2,1)}, u32[]{:S(2)}) copy-start(bf16[256,768]{1,0:T(8,128)(2,1)} %param.17) | copy-start | bytes 1179652
  132.5 43.7 %copy-start.3 = (bf16[768,128]{1,0:T(8,128)(2,1)S(1)}, bf16[768,128]{1,0:T(8,128)(2,1)}, u32[]{:S(2)}) copy-start(bf16[768,128]{1,0:T(8,128)(2,1)} %param.22) | copy-start | bytes 589828
  132.5 43.7 %copy-start.5 = (f32[768]{0:T(1024)S(1)}, f32[768]{0:T(1024)}, u32[]{:S(2)}) copy-start(f32[768]{0:T(1024)} %param.20) | copy-start | bytes 9220
  167.9 6.7 %collective-permute-start = (bf16[48,2048]{1,0:T(8,128)(2,1)S(1)}, bf16[48,2048]{1,0:T(8,128)(2,1)S(1)}, u32[]{:S(2)}, u32[]{:S(2)}) collective-permute-start(bf16[48,2048]{1,0:T(8,128)(2,1)S(1)} %fusion), channel_id=1, source_target_pairs={{0,1},{1,2},{2,3},{3,4},{4,5},{5,6},{6,7},{7,8},{8,9},{9,10},{10,1... | collective-permute-start | bytes 589832
  169.3 5.3 %collective-permute-start.1 = (bf16[42,2048]{1,0:T(8,128)(2,1)S(1)}, bf16[42,2048]{1,0:T(8,128)(2,1)S(1)}, u32[]{:S(2)}, u32[]{:S(2)}) collective-permute-start(bf16[42,2048]{1,0:T(8,128)(2,1)S(1)} %slice.44), channel_id=1, source_target_pairs={{0,2},{1,3},{2,4},{3,5},{4,6},{5,7},{6,8},{7,9},{8,10},{9,11},{10,... | collective-permute-start | bytes 516104
  225.6 125.8 %all-to-all-start.1 = ((bf16[32,21,2048]{2,1,0:T(8,128)(2,1)}), bf16[32,21,2048]{2,1,0:T(8,128)(2,1)}, u32[]{:S(2)}, u32[]{:S(2)}) async-start(bf16[32,21,2048]{2,1,0:T(8,128)(2,1)} %reshape.280), calls=%async_computation.3 | async-start | bytes 6291456 | tf_op jit(solution)/shard_map/all_to_all | solution.py:191
  236.1 52.0 %reduce-scatter.5.cloned.1.call-start = ((), (), s32[]{:S(2)}) async-start(), calls=%async_computation.5 | async-start | bytes 1179648 | tf_op jit(solution)/shard_map/reduce_scatter | solution.py:39
  236.3 4.7 %copy-start.7 = (bf16[128,2048]{1,0:T(8,128)(2,1)S(1)}, bf16[128,2048]{1,0:T(8,128)(2,1)}, u32[]{:S(2)}) copy-start(bf16[128,2048]{1,0:T(8,128)(2,1)} %param.26) | copy-start | bytes 1572868
  241.0 68.1 %copy-start.6 = (f32[128,4]{0,1:T(4,128)S(1)}, f32[128,4]{0,1:T(4,128)}, u32[]{:S(2)}) copy-start(f32[128,4]{0,1:T(4,128)} %param.30) | copy-start | bytes 6148
  248.5 57.0 %reduce-scatter.7.cloned.1.call-start = ((), (), s32[]{:S(2)}) async-start(), calls=%async_computation.6 | async-start | bytes 196608 | tf_op jit(solution)/shard_map/reduce_scatter | solution.py:39
  288.1 63.2 %all-gather.7.cloned.1.call-start = ((), (), s32[]{:S(2)}) async-start(), calls=%async_computation.7 | async-start | bytes 1179648 | tf_op jit(solution)/shard_map/all_gather | solution.py:46
Sparse Core Ops, SparseCore 0:
  15.4 132.1 all-gather.4
  176.3 43.9 all-gather.8
  248.6 39.4 reduce-scatter.4
  290.7 14.8 reduce-scatter.6
  309.2 42.0 all-gather.6
where the time goes:
time: 366 us; the launch traced here: 365 us
  blocking collectives  136 us (37%)
  waiting for transfers between devices  132 us (36%)
  matrix products  36.3 us (10%)
  local copies, waits for them, and re-layouts  20.5 us (6%)
  between operations  14.7 us (4%)
  starting transfers between devices  13.5 us (4%)
  other arithmetic  11.2 us (3%)
    all_to_all x1, blocking collectives, expert_part(): lax.all_to_all(outgoing, 'ep', split_axis=0, concat_axis=0, tiled=True)  97.5 us
    reduce_scatter x2, waiting for transfers between devices, sum_in_order(): pieces = lax.psum_scatter(pieces, axes[k], scatter_dimension=0, tiled=True)  56.9 us
    all_gather x1, waiting for transfers between devices, gather_in_order(): pieces = lax.all_gather(pieces, axes[k], axis=0, tiled=True)  42.1 us
    unnamed x1, blocking collectives  35.4 us
    all_gather x1, waiting for transfers between devices, sum_by_parts_2(): whole = lax.all_gather(own, axis, axis=0, tiled=True)  30.8 us
    all_to_all x1, starting transfers between devices, expert_part(): lax.all_to_all(summed, 'ep', split_axis=0, concat_axis=0, tiled=True)  10.6 us
    dot_general x1, matrix products, mixer_part(): jnp.dot(heads_out, mixer_out_weight, preferred_element_type=jnp.float32)  7.46 us
  transfers between devices with their start and end apart: 8, of which 5 were waited for; matrix products, arithmetic and copies ran while one was open for 23% of the time, Pallas kernels for 0%

commit v1 on v0

--- a/solution.py
+++ b/solution.py
@@ -62,7 +62,9 @@
     lines = shard.reshape(-1, *shard.shape[1:][-1:])
     padded = padded_to(lines, lax.axis_size(axis))
     own = lax.psum_scatter(padded, axis, scatter_dimension=0, tiled=True)
-    whole = lax.all_gather(own, axis, axis=0, tiled=True)
+    whole = jnp.concatenate(
+        lax.all_to_all(jnp.stack([own] * lax.axis_size(axis)), axis, 0, 0), axis=0
+    )
     return whole[: len(lines)].reshape(shard.shape)
 
 

time: 366 us -> 390 us (1.066)
  waiting for transfers between devices: 132 us -> 235 us
  blocking collectives: 136 us -> 39.7 us
  starting transfers between devices: 13.5 us -> 34.6 us
    all_to_all x0 -> x2, waiting for transfers between devices: none -> 133 us  [the longest x1 74.9 us: expert_part(): lax.all_to_all(outgoing, 'ep', split_axis=0, concat_axis=0, tiled=True)]
    all_to_all x1 -> x0, blocking collectives: 97.5 us -> none  [expert_part(): lax.all_to_all(outgoing, 'ep', split_axis=0, concat_axis=0, tiled=True)]
    all_gather x1 -> x0, waiting for transfers between devices: 30.8 us -> none  [sum_by_parts_2(): whole = lax.all_gather(own, axis, axis=0, tiled=True)]
    all_to_all x0 -> x2, starting transfers between devices: none -> 23.6 us  [the longest x1 13.7 us: expert_part(): lax.all_to_all(outgoing, 'ep', split_axis=0, concat_axis=0, tiled=True)]
  transfers between devices with their start and end apart: 8 -> 9, of which waited for: 5 -> 6; matrix products, arithmetic and copies ran while one was open for 23% -> 20% of each run, Pallas kernels for 0% -> 0%
where the time goes in v1:
time: 390 us; the launch traced here: 389 us
  waiting for transfers between devices  235 us (60%)
  blocking collectives  39.7 us (10%)
  starting transfers between devices  34.6 us (9%)
  matrix products  33.3 us (9%)
  local copies, waits for them, and re-layouts  22 us (6%)
  between operations  14.8 us (4%)
  other arithmetic  9.49 us (2%)
    all_to_all x1, waiting for transfers between devices, expert_part(): lax.all_to_all(outgoing, 'ep', split_axis=0, concat_axis=0, tiled=True)  74.9 us
    all_to_all x1, waiting for transfers between devices, sum_by_parts_2(): lax.all_to_all(jnp.stack([own] * lax.axis_size(axis)), axis, 0, 0)  58.6 us
    reduce_scatter x2, waiting for transfers between devices, sum_in_order(): pieces = lax.psum_scatter(pieces, axes[k], scatter_dimension=0, tiled=True)  57.2 us
    all_gather x1, waiting for transfers between devices, gather_in_order(): pieces = lax.all_gather(pieces, axes[k], axis=0, tiled=True)  42.1 us
    unnamed x1, blocking collectives  36.2 us
    all_to_all x1, starting transfers between devices, expert_part(): lax.all_to_all(outgoing, 'ep', split_axis=0, concat_axis=0, tiled=True)  13.7 us
    all_to_all x1, starting transfers between devices, sum_by_parts_2(): lax.all_to_all(jnp.stack([own] * lax.axis_size(axis)), axis, 0, 0)  9.99 us
    all_to_all x1, starting transfers between devices, expert_part(): lax.all_to_all(summed, 'ep', split_axis=0, concat_axis=0, tiled=True)  8.03 us
  transfers between devices with their start and end apart: 9, of which 6 were waited for; matrix products, arithmetic and copies ran while one was open for 20% of the time, Pallas kernels for 0%

profile of v1, /device:TPU:2, one launch (start us, length us, event | category | flops | bytes accessed | tf_op | source)
XLA Modules:
  0.0 388.7 jit_solution(8071785335086545068)
XLA Ops:
  7.2 0.8 copy.44
  8.0 0.1 eq.42
  8.1 0.1 eq.38
  8.3 1.2 reduce-window.6
  9.4 0.2 slice_reduce_fusion
  9.7 0.1 fusion.62
  9.8 0.1 reduce_sum.60
  10.0 0.7 multiply_add_fusion
  10.7 0.2 fusion.11
  10.9 1.2 fusion.29
  12.1 2.0 convolution_convert_fusion.1
  14.1 2.5 reshape.282
  16.7 13.7 %all-to-all-start = ((bf16[32,21,2048]{2,1,0:T(8,128)(2,1)}), bf16[32,21,2048]{2,1,0:T(8,128)(2,1)}, u32[]{:S(2)}, u32[]{:S(2)}) async-start(bf16[32,21,2048]{2,1,0:T(8,128)(2,1)} %reshape.282), calls=%async_computation.2 | async-start | bytes 6291456 | tf_op jit(solution)/shard_map/all_to_all | solution.py:177
  30.5 0.1 fusion.36
  30.6 0.2 fusion.33
  30.8 0.3 convolution_bitcast_fusion.2
  31.2 0.2 fusion.85
  31.4 0.3 convolution_convert_fusion.4
  31.7 0.3 convolution_convert_fusion.5
  32.0 0.7 pad_maximum_fusion
  32.7 74.9 %all-to-all-done = bf16[32,21,2048]{2,1,0:T(8,128)(2,1)} async-done(((bf16[32,21,2048]{2,1,0:T(8,128)(2,1)}), bf16[32,21,2048]{2,1,0:T(8,128)(2,1)}, u32[]{:S(2)}, u32[]{:S(2)}) %all-to-all-start) | async-done | bytes 2752544 | tf_op jit(solution)/shard_map/all_to_all | solution.py:177
  107.6 3.0 reshape.283
  110.6 2.7 convolution_minimum_fusion
  113.3 5.6 %convolution_convert_fusion = bf16[672,2048]{1,0:T(8,128)(2,1)} fusion(bf16[672,2048]{1,0:T(8,128)(2,1)S(1)} %reshape.283, bf16[1,128,2048]{2,1,0:T(8,128)(2,1)S(1)} %copy-done, bf16[1,2048,128]{2,1,0:T(8,128)(2,1)} %param.32, f32[672,128]{1,0:T(8,128)} %convolution_minimum_fusion), kind=kOutput, calls=%fused_computation.11 | convolution fusion | flops 706793472 | bytes 6897664 | tf_op jit(solution)/shard_map/dot_general | solution.py:190
  118.9 36.2 %fusion = bf16[48,2048]{1,0:T(8,128)(2,1)S(1)} fusion(bf16[672,2048]{1,0:T(8,128)(2,1)} %convolution_convert_fusion), kind=kCustom, calls=%all-reduce-scatter | all-reduce-scatter fusion | flops 1572865 | bytes 2951168
  155.1 1.3 collective-permute-start
  156.4 1.3 collective-permute-start.1
  157.8 1.3 dynamic-slice.4
  159.7 2.1 collective-permute-done.1
  161.8 0.8 concatenate.30
  162.6 2.0 stack.2
  164.7 10.0 %all-to-all-start.1 = ((bf16[16,42,2048]{2,1,0:T(8,128)(2,1)}), bf16[16,42,2048]{2,1,0:T(8,128)(2,1)}, u32[]{:S(2)}, u32[]{:S(2)}) async-start(bf16[16,42,2048]{2,1,0:T(8,128)(2,1)} %stack.2), calls=%async_computation.3 | async-start | bytes 6291456 | tf_op jit(solution)/shard_map/all_to_all | solution.py:66
  174.7 6.3 %convolution_bitcast_fusion.1 = f32[1,256,8192]{2,1,0:T(8,128)} fusion(bf16[8192,320]{0,1:T(8,128)(2,1)} %all-gather.3.cloned.1.call-done, bf16[768,128]{1,0:T(8,128)(2,1)S(1)} %copy-done.4, bf16[256,768]{1,0:T(8,128)(2,1)S(1)} %copy-done.2, f32[768]{0:T(1024)S(1)} %copy-done.6, f32[256]{0:T(256)S(1)} %add_rsqrt_fusion.1), kind=kOutput, calls=%fused_computation.1 | convolution fusion | flops 588021760 | bytes 11079680 | tf_op jit(solution)/shard_map/qhd,khd->hqk/dot_general | solution.py:124
  181.0 6.9 %fusion.96 = (f32[256]{0:T(256)S(1)}, f32[1,256,8192]{2,1,0:T(8,128)}) fusion(f32[1,256,8192]{2,1,0:T(8,128)} %convolution_bitcast_fusion.1, bf16[256,32]{0,1:T(8,128)(2,1)S(1)} %get-tuple-element.3, bf16[256,32]{0,1:T(8,128)(2,1)S(1)} %get-tuple-element.2, bf16[8192,320]{0,1:T(8,128)(2,1)} %all-gather.3.cloned.1.call-done, s32[256]{0:T(256)S(1)} %iota_add_fusion), kind=kOutput, calls=%fused_computation.113 | convolution fusion | flops 278986496 | bytes 17860608 | tf_op jit(solution)/shard_map/qhr,kr->hqk/dot_general | solution.py:125
  188.0 58.6 %all-to-all-done.1 = bf16[16,42,2048]{2,1,0:T(8,128)(2,1)} async-done(((bf16[16,42,2048]{2,1,0:T(8,128)(2,1)}), bf16[16,42,2048]{2,1,0:T(8,128)(2,1)}, u32[]{:S(2)}, u32[]{:S(2)}) %all-to-all-start.1) | async-done | bytes 2752544 | tf_op jit(solution)/shard_map/all_to_all | solution.py:66
  246.5 5.3 %reshape.284 = bf16[32,21,2048]{2,1,0:T(8,128)(2,1)} reshape(bf16[16,42,2048]{2,1,0:T(8,128)(2,1)} %all-to-all-done.1) | data formatting | bytes 5505024 | tf_op jit(solution)/shard_map/reshape | solution.py:192
  251.9 8.0 %all-to-all-start.2 = ((bf16[32,21,2048]{2,1,0:T(8,128)(2,1)}), bf16[32,21,2048]{2,1,0:T(8,128)(2,1)}, u32[]{:S(2)}, u32[]{:S(2)}) async-start(bf16[32,21,2048]{2,1,0:T(8,128)(2,1)} %reshape.284), calls=%async_computation.4 | async-start | bytes 6291456 | tf_op jit(solution)/shard_map/all_to_all | solution.py:193
  259.9 0.2 reduce-scatter.5.cloned.1.call-start
  260.2 4.7 %fusion.4 = f32[256]{0:T(256)S(1)} fusion(f32[1,256,8192]{2,1,0:T(8,128)} %get-tuple-element.9, f32[256]{0:T(256)S(1)} %broadcast_maximum_fusion, s32[256]{0:T(256)S(1)} %iota_add_fusion), kind=kLoop, calls=%fused_computation.7 | loop fusion | flops 8388352 | bytes 8391680 | tf_op jit(solution)/shard_map/reduce_sum | solution.py:134
  264.9 7.5 %convolution_convert_fusion.2 = bf16[256,2048]{1,0:T(8,128)(2,1)} fusion(bf16[128,2048]{1,0:T(8,128)(2,1)S(1)} %copy-done.8, bf16[8192,320]{0,1:T(8,128)(2,1)} %all-gather.3.cloned.1.call-done, f32[1,256,8192]{2,1,0:T(8,128)} %get-tuple-element.9, f32[256]{0:T(256)S(1)} %broadcast_maximum_fusion, s32[256]{0:T(256)S(1)} %iota_add_fusion, f32[256]{0:T(256)S(1)} %fusion.4), kind=kOutput, calls=%fused_computation.13 | convolution fusion | flops 680067072 | bytes 12061696 | tf_op jit(solution)/shard_map/dot_general | solution.py:146
  272.4 39.7 %reduce-scatter.5.cloned.1.call-done = bf16[2,16,2048]{2,1,0:T(8,128)(2,1)} async-done(((bf16[16,16,2048]{2,1,0:T(8,128)(2,1)}), bf16[2,16,2048]{2,1,0:T(8,128)(2,1)}) %reduce-scatter.5.cloned.1.call-update) | async-done | bytes 131088 | tf_op jit(solution)/shard_map/reduce_scatter | solution.py:39
  312.1 17.5 %reduce-scatter.7.cloned.1.call-done = bf16[1,16,2048]{2,1,0:T(8,128)(2,1)} async-done(((bf16[2,16,2048]{2,1,0:T(8,128)(2,1)}), bf16[1,16,2048]{2,1,0:T(8,128)(2,1)}) %reduce-scatter.7.cloned.1.call-update) | async-done | bytes 65552 | tf_op jit(solution)/shard_map/reduce_scatter | solution.py:39
  329.6 3.6 all_gather.10
  333.2 0.1 select_reduce_fusion
  333.4 42.1 %all-gather.5.cloned.1.call-done = bf16[16,16,2048]{2,1,0:T(8,128)(2,1)} async-done(((bf16[2,16,2048]{2,1,0:T(8,128)(2,1)}), bf16[16,16,2048]{2,1,0:T(8,128)(2,1)}) %all-gather.5.cloned.1.call-update) | async-done | bytes 1048592 | tf_op jit(solution)/shard_map/all_gather | solution.py:46
  375.4 3.0 reshape.285
  378.5 1.4 fusion.97
  379.9 2.3 copy.52
  (50 shorter events, 0.6 us)
Async XLA Ops:
  7.2 106.1 %copy-start = (bf16[1,128,2048]{2,1,0:T(8,128)(2,1)S(1)}, bf16[1,128,2048]{2,1,0:T(8,128)(2,1)}, u32[]{:S(2)}) copy-start(bf16[1,128,2048]{2,1,0:T(8,128)(2,1)} %param.33) | copy-start | bytes 1572868
  16.6 13.8 %copy-start.3 = (bf16[256,512]{1,0:T(8,128)(2,1)S(1)}, bf16[256,512]{1,0:T(8,128)(2,1)}, u32[]{:S(2)}) copy-start(bf16[256,512]{1,0:T(8,128)(2,1)} %param.18) | copy-start | bytes 786436
  16.6 13.9 %copy-start.1 = (bf16[256,768]{1,0:T(8,128)(2,1)S(1)}, bf16[256,768]{1,0:T(8,128)(2,1)}, u32[]{:S(2)}) copy-start(bf16[256,768]{1,0:T(8,128)(2,1)} %param.17) | copy-start | bytes 1179652
  16.6 14.1 %copy-start.6 = (f32[768]{0:T(1024)S(1)}, f32[768]{0:T(1024)}, u32[]{:S(2)}) copy-start(f32[768]{0:T(1024)} %param.20) | copy-start | bytes 9220
  16.7 14.1 %copy-start.11 = (bf16[768,64]{0,1:T(8,128)(2,1)S(1)}, bf16[768,64]{0,1:T(8,128)(2,1)}, u32[]{:S(2)}) copy-start(bf16[768,64]{0,1:T(8,128)(2,1)} %param.23) | copy-start | bytes 294916
  16.7 14.5 %copy-start.5 = (bf16[256,64]{0,1:T(8,128)(2,1)S(1)}, bf16[256,64]{0,1:T(8,128)(2,1)}, u32[]{:S(2)}) copy-start(bf16[256,64]{0,1:T(8,128)(2,1)} %param.19) | copy-start | bytes 98308
  16.7 14.7 %copy-start.9 = (bf16[512,128]{1,0:T(8,128)(2,1)S(1)}, bf16[512,128]{1,0:T(8,128)(2,1)}, u32[]{:S(2)}) copy-start(bf16[512,128]{1,0:T(8,128)(2,1)} %param.25) | copy-start | bytes 393220
  16.7 14.7 %copy-start.12 = (f32[512]{0:T(512)S(1)}, f32[512]{0:T(512)}, u32[]{:S(2)}) copy-start(f32[512]{0:T(512)} %param.21) | copy-start | bytes 6148
  16.7 15.0 %copy-start.10 = (bf16[512,128]{1,0:T(8,128)(2,1)S(1)}, bf16[512,128]{1,0:T(8,128)(2,1)}, u32[]{:S(2)}) copy-start(bf16[512,128]{1,0:T(8,128)(2,1)} %param.24) | copy-start | bytes 393220
  16.7 90.9 %all-to-all-start = ((bf16[32,21,2048]{2,1,0:T(8,128)(2,1)}), bf16[32,21,2048]{2,1,0:T(8,128)(2,1)}, u32[]{:S(2)}, u32[]{:S(2)}) async-start(bf16[32,21,2048]{2,1,0:T(8,128)(2,1)} %reshape.282), calls=%async_computation.2 | async-start | bytes 6291456 | tf_op jit(solution)/shard_map/all_to_all | solution.py:177
  30.4 144.3 %all-gather.3.cloned.1.call-start = ((), (), s32[]{:S(2)}) async-start(), calls=%async_computation.5 | async-start | bytes 5406720 | tf_op jit(solution)/shard_map/all_gather | solution.py:21
  155.1 6.7 %collective-permute-start = (bf16[48,2048]{1,0:T(8,128)(2,1)S(1)}, bf16[48,2048]{1,0:T(8,128)(2,1)S(1)}, u32[]{:S(2)}, u32[]{:S(2)}) collective-permute-start(bf16[48,2048]{1,0:T(8,128)(2,1)S(1)} %fusion), channel_id=1, source_target_pairs={{0,1},{1,2},{2,3},{3,4},{4,5},{5,6},{6,7},{7,8},{8,9},{9,10},{10,1... | collective-permute-start | bytes 589832
  156.4 5.3 %collective-permute-start.1 = (bf16[42,2048]{1,0:T(8,128)(2,1)S(1)}, bf16[42,2048]{1,0:T(8,128)(2,1)S(1)}, u32[]{:S(2)}, u32[]{:S(2)}) collective-permute-start(bf16[42,2048]{1,0:T(8,128)(2,1)S(1)} %slice.44), channel_id=1, source_target_pairs={{0,2},{1,3},{2,4},{3,5},{4,6},{5,7},{6,8},{7,9},{8,10},{9,11},{10,... | collective-permute-start | bytes 516104
  162.6 12.1 %copy-start.2 = (bf16[256,768]{1,0:T(8,128)(2,1)S(1)}, bf16[256,768]{1,0:T(8,128)(2,1)}, u32[]{:S(2)}) copy-start(bf16[256,768]{1,0:T(8,128)(2,1)} %param.17) | copy-start | bytes 1179652
  162.6 12.1 %copy-start.4 = (bf16[768,128]{1,0:T(8,128)(2,1)S(1)}, bf16[768,128]{1,0:T(8,128)(2,1)}, u32[]{:S(2)}) copy-start(bf16[768,128]{1,0:T(8,128)(2,1)} %param.22) | copy-start | bytes 589828
  164.7 81.9 %all-to-all-start.1 = ((bf16[16,42,2048]{2,1,0:T(8,128)(2,1)}), bf16[16,42,2048]{2,1,0:T(8,128)(2,1)}, u32[]{:S(2)}, u32[]{:S(2)}) async-start(bf16[16,42,2048]{2,1,0:T(8,128)(2,1)} %stack.2), calls=%async_computation.3 | async-start | bytes 6291456 | tf_op jit(solution)/shard_map/all_to_all | solution.py:66
  251.9 123.5 %all-to-all-start.2 = ((bf16[32,21,2048]{2,1,0:T(8,128)(2,1)}), bf16[32,21,2048]{2,1,0:T(8,128)(2,1)}, u32[]{:S(2)}, u32[]{:S(2)}) async-start(bf16[32,21,2048]{2,1,0:T(8,128)(2,1)} %reshape.284), calls=%async_computation.4 | async-start | bytes 6291456 | tf_op jit(solution)/shard_map/all_to_all | solution.py:193
  259.9 52.1 %reduce-scatter.5.cloned.1.call-start = ((), (), s32[]{:S(2)}) async-start(), calls=%async_computation.6 | async-start | bytes 1179648 | tf_op jit(solution)/shard_map/reduce_scatter | solution.py:39
  260.2 4.7 %copy-start.8 = (bf16[128,2048]{1,0:T(8,128)(2,1)S(1)}, bf16[128,2048]{1,0:T(8,128)(2,1)}, u32[]{:S(2)}) copy-start(bf16[128,2048]{1,0:T(8,128)(2,1)} %param.26) | copy-start | bytes 1572868
  264.8 68.4 %copy-start.7 = (f32[128,4]{0,1:T(4,128)S(1)}, f32[128,4]{0,1:T(4,128)}, u32[]{:S(2)}) copy-start(f32[128,4]{0,1:T(4,128)} %param.30) | copy-start | bytes 6148
  272.3 57.3 %reduce-scatter.7.cloned.1.call-start = ((), (), s32[]{:S(2)}) async-start(), calls=%async_computation.7 | async-start | bytes 196608 | tf_op jit(solution)/shard_map/reduce_scatter | solution.py:39
  312.1 63.3 %all-gather.5.cloned.1.call-start = ((), (), s32[]{:S(2)}) async-start(), calls=%async_computation.8 | async-start | bytes 1179648 | tf_op jit(solution)/shard_map/all_gather | solution.py:46
Sparse Core Ops, SparseCore 0:
  34.8 121.5 all-gather.2
  272.5 39.5 reduce-scatter.4
  314.8 14.7 reduce-scatter.6
  333.3 42.0 all-gather.4
